TPU v7x, 128 devices: a whole 4x4x4 slice. The times are simulated.
128 devices in a mesh: ra: 16 (over z, x), cb: 8 (over y, core).
Axes of the slice: x: 4, y: 4, z: 4, core: 2. Of those that a mesh axis runs over, the one named last changes fastest.
Arguments:
- inputs: bfloat16 [1536, 4096], P(None, 'ra'), may hold values from -12 to 12
- gate_weight: bfloat16 [2, 4096, 11264], P(None, 'ra', 'cb'), may hold values from -0.09375 to 0.09375
- up_weight: bfloat16 [2, 4096, 11264], P(None, 'ra', 'cb'), may hold values from -0.09375 to 0.09375
- down_weight: bfloat16 [2, 11264, 4096], P(None, 'cb', 'ra'), may hold values from -0.0546875 to 0.0546875
- norm_gain: float32 [2, 4096], P(None, 'ra'), may hold values from 0.05 to 8
- norm_shift: float32 [2, 4096], P(None, 'ra'), may hold values from -1.5 to 1.5
Outputs:
- outputs: bfloat16 [1536, 4096], P(None, 'ra')
All inputs are finite; a program needn't handle non-finite values.
Results may differ from a plain program's by a relative error of at most 0.04.
Values may be sent and summed in bfloat16 or wider, within the bound.
No kernel may reach another device: no remote copies, remote signals or barrier semaphores. Data moves between devices by JAX's collectives and lax.ppermute only.
A program may use at most 64 MiB of HBM per device.

v0:
```python
import jax
import jax.numpy as jnp
from jax import lax
from jax.sharding import Mesh
from jax.sharding import PartitionSpec as P

RESIDUAL = 0.5
EPSILON = 1e-05
BF16 = jnp.bfloat16
F32 = jnp.float32


def exchange(parts, axes):
    return lax.all_to_all(parts, axes, 0, 0, tiled=True)


def share(block, axes, peers):
    return exchange(jnp.broadcast_to(block[None], (peers, *block.shape)), axes)


def swap_core(block):
    return lax.ppermute(block, "c", [(0, 1), (1, 0)])


def dot_nt(a, b):
    return lax.dot_general(a, b, (((1,), (1,)), ((), ())), preferred_element_type=F32)


def regroup_weights(gate, up, down):
    stacked = jnp.stack((gate.T, up.T, down))
    rows = stacked.shape[1] // 4
    parts = stacked.reshape(3, 4, rows, 256).transpose(1, 0, 2, 3)
    mine = exchange(parts, "x")
    mine = mine.transpose(1, 2, 0, 3).reshape(3, rows, 1024)
    other = swap_core(mine)
    both = jnp.concatenate((mine, other), axis=1)
    return (both[:2].reshape(2 * 2 * rows, 1024), both[2])


def normed(mixed, row_sum, row_squares, gain, shift):
    mean = row_sum / 4096.0
    var = row_squares / 4096.0 - mean * mean
    out = (mixed - mean[:, None]) * lax.rsqrt(var + EPSILON)[:, None]
    return (out * gain + shift).astype(BF16)


def hidden_units(stream, w_gu):
    partial = dot_nt(stream, w_gu).astype(BF16)
    cols = partial.shape[1] // 2
    summed = exchange(partial.reshape(4, -1, 2 * cols), "z").astype(F32).sum(axis=0)
    hidden = (jax.nn.silu(summed[:, :cols]) * summed[:, cols:]).astype(BF16)
    return share(hidden, "z", 4).reshape(-1, cols)


def per_device(inputs, gate_weight, up_weight, down_weight, norm_gain, norm_shift):
    c = lax.axis_index("c")
    x = lax.axis_index("x")
    y = lax.axis_index("y")
    half = inputs.shape[0] // 2
    quarter = half // 4
    mine = lax.dynamic_slice_in_dim(inputs, c * half + y * quarter, quarter, 0)
    rows = share(mine, "x", 4).transpose(1, 0, 2).reshape(quarter, 1024)
    stream = share(rows, "y", 4).reshape(half, 1024)
    affine = jnp.stack((norm_gain[0], norm_shift[0]))
    affine = lax.all_gather(affine, "x", axis=1, tiled=True)
    gu0, down0 = regroup_weights(gate_weight[0], up_weight[0], down_weight[0])
    gu1, down1 = regroup_weights(gate_weight[1], up_weight[1], down_weight[1])
    hidden = hidden_units(stream, gu0)
    partial = jnp.dot(hidden, down0, preferred_element_type=F32).astype(BF16)
    block = half // 16
    branch = exchange(partial.reshape(16, block, 1024), ("x", "y")).astype(F32).sum(axis=0)
    own = lax.dynamic_slice_in_dim(stream, (x * 4 + y) * block, block, 0)
    mixed = RESIDUAL * own.astype(F32) + branch
    stats = lax.psum(jnp.stack((mixed.sum(axis=1), (mixed * mixed).sum(axis=1))), "z")
    out = normed(mixed, stats[0], stats[1], affine[0], affine[1])
    stream = share(out, ("x", "y"), 16).reshape(half, 1024)
    hidden = hidden_units(stream, gu1)
    partial = jnp.dot(hidden, down1, preferred_element_type=F32).astype(BF16)
    parts = partial.reshape(4, quarter, 4, 256).transpose(2, 0, 1, 3).reshape(16, quarter, 256)
    branch = exchange(parts, ("x", "y")).astype(F32).sum(axis=0)
    own = lax.dynamic_slice(stream, (y * quarter, x * 256), (quarter, 256))
    mixed = RESIDUAL * own.astype(F32) + branch
    stats = lax.psum(jnp.stack((mixed.sum(axis=1), (mixed * mixed).sum(axis=1))), ("z", "x"))
    out = normed(mixed, stats[0], stats[1], norm_gain[1], norm_shift[1])
    ours = share(out, "y", 4).reshape(half, 256)
    theirs = swap_core(ours)
    result = jnp.concatenate((ours, theirs), axis=0)
    swapped = jnp.concatenate((theirs, ours), axis=0)
    return jnp.where(c == 0, result, swapped)


def solution(mesh):
    finer = Mesh(mesh.devices.reshape(4, 4, 4, 2), ("z", "x", "y", "c"))
    ra, cb = (("z", "x"), ("y", "c"))
    in_specs = (
        P(None, ra),
        P(None, ra, cb),
        P(None, ra, cb),
        P(None, cb, ra),
        P(None, ra),
        P(None, ra),
    )
    return jax.shard_map(
        per_device, mesh=finer, in_specs=in_specs, out_specs=P(None, ra), check_vma=False
    )
```

profile of v0, /device:TPU:1, one launch (start us, length us, event | category | flops | bytes accessed | tf_op | source)
XLA Modules:
  0.0 365.9 jit_solution(2115882943331297913)
XLA Ops:
  0.0 2.4 fusion.6
  2.4 0.3 copy.37
  2.7 2.3 fusion.7
  5.0 0.3 copy.38
  5.2 2.3 fusion.8
  7.5 0.2 maximum_bitcast_fusion
  7.9 30.5 %all_to_all.60 = bf16[4,3,352,256]{3,2,1,0:T(8,128)(2,1)S(1)} all-to-all(bf16[4,3,352,256]{3,2,1,0:T(8,128)(2,1)S(1)} %copy.30), channel_id=1, replica_groups=mesh['z'=4,'x'=4,'y'=4,'c'=2] {'x'}, dimensions={0} | all-to-all | bytes 4325376 | tf_op jit(solution)/shard_map/all_to_all | solution.py:14
  38.4 0.3 copy.42
  38.7 2.2 collective-permute-start
  41.0 10.2 %all_to_all.61 = bf16[4,192,256]{2,1,0:T(8,128)(2,1)S(1)} all-to-all(bf16[4,192,256]{2,1,0:T(8,128)(2,1)S(1)} %broadcast_in_dim.14), channel_id=1, replica_groups=mesh['z'=4,'x'=4,'y'=4,'c'=2] {'x'}, dimensions={0} | all-to-all | bytes 786432 | tf_op jit(solution)/shard_map/all_to_all | solution.py:14
  51.2 1.4 broadcast_in_dim.16
  52.7 4.4 %all-to-all-start.1 = ((bf16[4,192,1024]{2,1,0:T(8,128)(2,1)}), bf16[4,192,1024]{2,1,0:T(8,128)(2,1)}, u32[]{:S(2)}, u32[]{:S(2)}) async-start(bf16[4,192,1024]{2,1,0:T(8,128)(2,1)} %broadcast_in_dim.16), calls=%async_computation.1 | async-start | bytes 3145728 | tf_op jit(solution)/shard_map/all_to_all | solution.py:14
  57.0 0.2 constant_dynamic-update-slice_fusion.1
  57.2 1.8 constant_dynamic-update-slice_fusion
  59.0 2.0 copy-done.2
  61.1 1.9 slice.96
  62.9 13.6 %all-to-all-done.1 = bf16[4,192,1024]{2,1,0:T(8,128)(2,1)} async-done(((bf16[4,192,1024]{2,1,0:T(8,128)(2,1)}), bf16[4,192,1024]{2,1,0:T(8,128)(2,1)}, u32[]{:S(2)}, u32[]{:S(2)}) %all-to-all-start.1) | async-done | bytes 1572896 | tf_op jit(solution)/shard_map/all_to_all | solution.py:14
  76.5 4.9 %convolution_convert_fusion.1 = bf16[768,1408]{1,0:T(8,128)(2,1)S(1)} fusion(bf16[768,1024]{1,0:T(8,128)(2,1)} %bitcast.1, bf16[1408,1024]{1,0:T(8,128)(2,1)} %bitcast.85), kind=kOutput, calls=%fused_computation.3 | convolution fusion | flops 2215673856 | bytes 6619136 | tf_op jit(solution)/shard_map/dot_general | solution.py:26
  81.5 29.2 %all_to_all.62 = bf16[4,192,1408]{2,1,0:T(8,128)(2,1)S(1)} all-to-all(bf16[4,192,1408]{2,1,0:T(8,128)(2,1)S(1)} %bitcast.93), channel_id=1, replica_groups=mesh['z'=4,'x'=4,'y'=4,'c'=2] {'z'}, dimensions={0} | all-to-all | bytes 4325376 | tf_op jit(solution)/shard_map/all_to_all | solution.py:14
  110.7 0.3 convert_reduce_fusion.1
  111.0 0.2 fusion.1
  111.2 1.2 broadcast_in_dim.17
  112.4 4.4 %all-to-all-start.4 = ((bf16[4,192,704]{2,1,0:T(8,128)(2,1)}), bf16[4,192,704]{2,1,0:T(8,128)(2,1)}, u32[]{:S(2)}, u32[]{:S(2)}) async-start(bf16[4,192,704]{2,1,0:T(8,128)(2,1)} %broadcast_in_dim.17), calls=%async_computation.4 | async-start | bytes 2359296 | tf_op jit(solution)/shard_map/all_to_all | solution.py:14
  116.8 0.3 copy.39
  117.1 0.3 copy.40
  117.4 0.2 maximum_bitcast_fusion.1
  117.6 1.5 copy.34
  119.1 10.4 %all-to-all-done.4 = bf16[4,192,704]{2,1,0:T(8,128)(2,1)} async-done(((bf16[4,192,704]{2,1,0:T(8,128)(2,1)}), bf16[4,192,704]{2,1,0:T(8,128)(2,1)}, u32[]{:S(2)}, u32[]{:S(2)}) %all-to-all-start.4) | async-done | bytes 1081376 | tf_op jit(solution)/shard_map/all_to_all | solution.py:14
  129.5 3.6 all-to-all-start.7
  133.2 4.3 %convolution_convert_fusion.3 = bf16[768,1024]{1,0:T(8,128)(2,1)} fusion(bf16[768,704]{1,0:T(8,128)(2,1)} %bitcast.13, bf16[3,704,1024]{2,1,0:T(8,128)(2,1)} %copy-done.2), kind=kOutput, calls=%fused_computation.9 | convolution fusion | flops 1108082688 | bytes 4194304 | tf_op jit(solution)/shard_map/dot_general | solution.py:69
  137.5 18.0 %all-to-all-done.7 = bf16[4,3,352,256]{3,2,1,0:T(8,128)(2,1)S(1)} async-done(((bf16[4,3,352,256]{3,2,1,0:T(8,128)(2,1)}), bf16[4,3,352,256]{3,2,1,0:T(8,128)(2,1)S(1)}, u32[]{:S(2)}, u32[]{:S(2)}) %all-to-all-start.7) | async-done | bytes 2162720 | tf_op jit(solution)/shard_map/all_to_all | solution.py:14
  155.5 4.4 %all-to-all-start.5 = ((bf16[16,48,1024]{2,1,0:T(8,128)(2,1)}), bf16[16,48,1024]{2,1,0:T(8,128)(2,1)}, u32[]{:S(2)}, u32[]{:S(2)}) async-start(bf16[16,48,1024]{2,1,0:T(8,128)(2,1)} %bitcast.95), calls=%async_computation.5 | async-start | bytes 3145728 | tf_op jit(solution)/shard_map/all_to_all | solution.py:14
  160.0 18.8 %all_gather.3 = f32[2,1024]{1,0:T(2,128)S(1)} all-gather(f32[2,256]{1,0:T(2,128)S(1)} %pad_maximum_fusion), channel_id=1, replica_groups=mesh['z'=4,'x'=4,'y'=4,'c'=2] {'x'}, dimensions={1}, use_global_device_ids=true | all-gather | bytes 10240 | tf_op jit(solution)/shard_map/all_gather | solution.py:65
  178.8 1.6 copy.43
  180.4 8.3 %collective-permute-start.1 = (bf16[3,352,1024]{2,1,0:T(8,128)(2,1)}, bf16[3,352,1024]{2,1,0:T(8,128)(2,1)S(1)}, u32[]{:S(2)}, u32[]{:S(2)}) collective-permute-start(bf16[3,352,1024]{2,1,0:T(8,128)(2,1)} %bitcast.59), channel_id=1, source_target_pairs={{0,1},{1,0},{2,3},{3,2},{4,5},{5,4},{6,7},{7,6},{8,9},{9,8},{10,11... | collective-permute-start | bytes 6488072 | tf_op jit(solution)/shard_map/ppermute | solution.py:22
  188.8 1.7 convert_reduce_fusion.3
  190.5 1.0 fusion.2
  191.5 6.9 %psum.14 = f32[2,48]{1,0:T(2,128)S(1)} all-reduce(f32[2,48]{1,0:T(2,128)S(1)} %pad_maximum_fusion.2), channel_id=1, replica_groups=mesh['z'=4,'x'=4,'y'=4,'c'=2] {'z'}, use_global_device_ids=true, to_apply=%region_4.5 | all-reduce | flops 96 | bytes 768 | tf_op jit(solution)/shard_map/psum | solution.py:74
  198.4 1.0 add_convert_fusion.1
  199.4 1.4 broadcast_in_dim.18
  200.8 5.1 %all-to-all-start.6 = ((bf16[16,48,1024]{2,1,0:T(8,128)(2,1)}), bf16[16,48,1024]{2,1,0:T(8,128)(2,1)}, u32[]{:S(2)}, u32[]{:S(2)}) async-start(bf16[16,48,1024]{2,1,0:T(8,128)(2,1)} %broadcast_in_dim.18), calls=%async_computation.6 | async-start | bytes 3145728 | tf_op jit(solution)/shard_map/all_to_all | solution.py:14
  205.9 1.8 constant_dynamic-update-slice_fusion.3
  207.7 0.2 constant_dynamic-update-slice_fusion.2
  207.9 2.0 copy-done.3
  209.9 1.9 slice.102
  211.8 14.5 %all-to-all-done.6 = bf16[16,48,1024]{2,1,0:T(8,128)(2,1)} async-done(((bf16[16,48,1024]{2,1,0:T(8,128)(2,1)}), bf16[16,48,1024]{2,1,0:T(8,128)(2,1)}, u32[]{:S(2)}, u32[]{:S(2)}) %all-to-all-start.6) | async-done | bytes 1572896 | tf_op jit(solution)/shard_map/all_to_all | solution.py:14
  226.3 4.9 %convolution_convert_fusion = bf16[768,1408]{1,0:T(8,128)(2,1)S(1)} fusion(bf16[768,1024]{1,0:T(8,128)(2,1)} %bitcast.22, bf16[1408,1024]{1,0:T(8,128)(2,1)} %bitcast.86), kind=kOutput, calls=%fused_computation.2 | convolution fusion | flops 2215673856 | bytes 6619136 | tf_op jit(solution)/shard_map/dot_general | solution.py:26
  231.3 25.4 %all_to_all.63 = bf16[4,192,1408]{2,1,0:T(8,128)(2,1)S(1)} all-to-all(bf16[4,192,1408]{2,1,0:T(8,128)(2,1)S(1)} %bitcast.94), channel_id=1, replica_groups=mesh['z'=4,'x'=4,'y'=4,'c'=2] {'z'}, dimensions={0} | all-to-all | bytes 4325376 | tf_op jit(solution)/shard_map/all_to_all | solution.py:14
  256.7 0.3 convert_reduce_fusion
  257.0 0.2 fusion
  257.4 13.7 %all_to_all.64 = bf16[4,192,704]{2,1,0:T(8,128)(2,1)S(1)} all-to-all(bf16[4,192,704]{2,1,0:T(8,128)(2,1)S(1)} %broadcast_in_dim.19), channel_id=1, replica_groups=mesh['z'=4,'x'=4,'y'=4,'c'=2] {'z'}, dimensions={0} | all-to-all | bytes 2162688 | tf_op jit(solution)/shard_map/all_to_all | solution.py:14
  271.1 3.9 %convolution_convert_fusion.2 = bf16[768,1024]{1,0:T(8,128)(2,1)} fusion(bf16[768,704]{1,0:T(8,128)(2,1)S(1)} %bitcast.100, bf16[3,704,1024]{2,1,0:T(8,128)(2,1)} %copy-done.3), kind=kOutput, calls=%fused_computation.8 | convolution fusion | flops 1108082688 | bytes 4096000 | tf_op jit(solution)/shard_map/dot_general | solution.py:78
  275.0 2.9 reshape.113
  277.9 1.4 copy.36
  279.3 10.2 %all-to-all-start.10 = ((bf16[16,192,256]{2,1,0:T(8,128)(2,1)}), bf16[16,192,256]{2,1,0:T(8,128)(2,1)S(1)}, u32[]{:S(2)}, u32[]{:S(2)}) async-start(bf16[16,192,256]{2,1,0:T(8,128)(2,1)} %bitcast.84), calls=%async_computation.10 | async-start | bytes 3145728 | tf_op jit(solution)/shard_map/all_to_all | solution.py:14
  289.6 19.0 %all-to-all-done.10 = bf16[16,192,256]{2,1,0:T(8,128)(2,1)S(1)} async-done(((bf16[16,192,256]{2,1,0:T(8,128)(2,1)}), bf16[16,192,256]{2,1,0:T(8,128)(2,1)S(1)}, u32[]{:S(2)}, u32[]{:S(2)}) %all-to-all-start.10) | async-done | bytes 1572896 | tf_op jit(solution)/shard_map/all_to_all | solution.py:14
  308.6 0.2 convert_reduce_fusion.2
  308.8 1.1 fusion.3
  309.9 31.9 %psum.15 = f32[2,192]{1,0:T(2,128)S(1)} all-reduce(f32[2,192]{1,0:T(2,128)S(1)} %pad_maximum_fusion.1), channel_id=1, replica_groups=mesh['z'=4,'x'=4,'y'=4,'c'=2] {'z','x'}, use_global_device_ids=true, to_apply=%region_9.10 | all-reduce | flops 384 | bytes 3072 | tf_op jit(solution)/shard_map/psum | solution.py:83
  341.9 1.0 add_convert_fusion
  342.9 10.1 %all_to_all.65 = bf16[4,192,256]{2,1,0:T(8,128)(2,1)S(1)} all-to-all(bf16[4,192,256]{2,1,0:T(8,128)(2,1)S(1)} %broadcast_in_dim.20), channel_id=1, replica_groups=mesh['z'=4,'x'=4,'y'=4,'c'=2] {'y'}, dimensions={0} | all-to-all | bytes 786432 | tf_op jit(solution)/shard_map/all_to_all | solution.py:14
  353.0 10.3 %collective-permute-start.2 = (bf16[768,256]{1,0:T(8,128)(2,1)S(1)}, bf16[768,256]{1,0:T(8,128)(2,1)S(1)}, u32[]{:S(2)}, u32[]{:S(2)}) collective-permute-start(bf16[768,256]{1,0:T(8,128)(2,1)S(1)} %bitcast.97), channel_id=1, source_target_pairs={{0,1},{1,0},{2,3},{3,2},{4,5},{5,4},{6,7},{7,6},{8,9},{9,8},{10,11... | collective-permute-start | bytes 1179656 | tf_op jit(solution)/shard_map/ppermute | solution.py:22
  363.3 1.3 collective-permute-done.2
  364.7 1.2 maximum_select_fusion
  (34 shorter events, 0.4 us)
Async XLA Ops:
  0.0 40.9 %copy-start = (bf16[1536,256]{1,0:T(8,128)(2,1)S(1)}, bf16[1536,256]{1,0:T(8,128)(2,1)}, u32[]{:S(2)}) copy-start(bf16[1536,256]{1,0:T(8,128)(2,1)} %param.6) | copy-start | bytes 2359300
  38.7 18.5 %collective-permute-start = (bf16[3,352,1024]{2,1,0:T(8,128)(2,1)S(1)}, bf16[3,352,1024]{2,1,0:T(8,128)(2,1)}, u32[]{:S(2)}, u32[]{:S(2)}) collective-permute-start(bf16[3,352,1024]{2,1,0:T(8,128)(2,1)S(1)} %bitcast.81), channel_id=1, source_target_pairs={{0,1},{1,0},{2,3},{3,2},{4,5},{5,4},{6,7},{7,6},{8,9},{9,8},{10,11... | collective-permute-start | bytes 6488072 | tf_op jit(solution)/shard_map/ppermute | solution.py:22
  52.7 23.9 %all-to-all-start.1 = ((bf16[4,192,1024]{2,1,0:T(8,128)(2,1)}), bf16[4,192,1024]{2,1,0:T(8,128)(2,1)}, u32[]{:S(2)}, u32[]{:S(2)}) async-start(bf16[4,192,1024]{2,1,0:T(8,128)(2,1)} %broadcast_in_dim.16), calls=%async_computation.1 | async-start | bytes 3145728 | tf_op jit(solution)/shard_map/all_to_all | solution.py:14
  59.0 2.1 copy-start.2
  111.2 5.6 %copy-start.4 = (bf16[1,256,1408]{2,1,0:T(8,128)(2,1)S(1)}, bf16[1,256,1408]{2,1,0:T(8,128)(2,1)}, u32[]{:S(2)}) copy-start(bf16[1,256,1408]{2,1,0:T(8,128)(2,1)} %get-tuple-element.9) | copy-start | bytes 2162692
  112.4 4.7 %copy-start.5 = (bf16[1,256,1408]{2,1,0:T(8,128)(2,1)S(1)}, bf16[1,256,1408]{2,1,0:T(8,128)(2,1)}, u32[]{:S(2)}) copy-start(bf16[1,256,1408]{2,1,0:T(8,128)(2,1)} %get-tuple-element.11) | copy-start | bytes 2162692
  112.4 5.0 %copy-start.6 = (bf16[1,1408,256]{2,1,0:T(8,128)(2,1)S(1)}, bf16[1,1408,256]{2,1,0:T(8,128)(2,1)}, u32[]{:S(2)}) copy-start(bf16[1,1408,256]{2,1,0:T(8,128)(2,1)} %get-tuple-element.13) | copy-start | bytes 2162692
  112.4 17.1 %all-to-all-start.4 = ((bf16[4,192,704]{2,1,0:T(8,128)(2,1)}), bf16[4,192,704]{2,1,0:T(8,128)(2,1)}, u32[]{:S(2)}, u32[]{:S(2)}) async-start(bf16[4,192,704]{2,1,0:T(8,128)(2,1)} %broadcast_in_dim.17), calls=%async_computation.4 | async-start | bytes 2359296 | tf_op jit(solution)/shard_map/all_to_all | solution.py:14
  129.5 25.9 %all-to-all-start.7 = ((bf16[4,3,352,256]{3,2,1,0:T(8,128)(2,1)}), bf16[4,3,352,256]{3,2,1,0:T(8,128)(2,1)S(1)}, u32[]{:S(2)}, u32[]{:S(2)}) async-start(bf16[4,3,352,256]{3,2,1,0:T(8,128)(2,1)} %copy.34), calls=%async_computation.7 | async-start | bytes 4325376 | tf_op jit(solution)/shard_map/all_to_all | solution.py:14
  137.5 22.4 %copy-start.7 = (f32[2,256]{1,0:T(2,128)S(1)}, f32[2,256]{1,0:T(2,128)}, u32[]{:S(2)}) copy-start(f32[2,256]{1,0:T(2,128)} %param.10) | copy-start | bytes 6148
  137.5 22.5 %copy-start.8 = (f32[2,256]{1,0:T(2,128)S(1)}, f32[2,256]{1,0:T(2,128)}, u32[]{:S(2)}) copy-start(f32[2,256]{1,0:T(2,128)} %param.11) | copy-start | bytes 6148
  155.5 33.3 %all-to-all-start.5 = ((bf16[16,48,1024]{2,1,0:T(8,128)(2,1)}), bf16[16,48,1024]{2,1,0:T(8,128)(2,1)}, u32[]{:S(2)}, u32[]{:S(2)}) async-start(bf16[16,48,1024]{2,1,0:T(8,128)(2,1)} %bitcast.95), calls=%async_computation.5 | async-start | bytes 3145728 | tf_op jit(solution)/shard_map/all_to_all | solution.py:14
  180.4 27.2 %collective-permute-start.1 = (bf16[3,352,1024]{2,1,0:T(8,128)(2,1)}, bf16[3,352,1024]{2,1,0:T(8,128)(2,1)S(1)}, u32[]{:S(2)}, u32[]{:S(2)}) collective-permute-start(bf16[3,352,1024]{2,1,0:T(8,128)(2,1)} %bitcast.59), channel_id=1, source_target_pairs={{0,1},{1,0},{2,3},{3,2},{4,5},{5,4},{6,7},{7,6},{8,9},{9,8},{10,11... | collective-permute-start | bytes 6488072 | tf_op jit(solution)/shard_map/ppermute | solution.py:22
  200.8 25.5 %all-to-all-start.6 = ((bf16[16,48,1024]{2,1,0:T(8,128)(2,1)}), bf16[16,48,1024]{2,1,0:T(8,128)(2,1)}, u32[]{:S(2)}, u32[]{:S(2)}) async-start(bf16[16,48,1024]{2,1,0:T(8,128)(2,1)} %broadcast_in_dim.18), calls=%async_computation.6 | async-start | bytes 3145728 | tf_op jit(solution)/shard_map/all_to_all | solution.py:14
  207.9 2.0 copy-start.3
  279.3 29.2 %all-to-all-start.10 = ((bf16[16,192,256]{2,1,0:T(8,128)(2,1)}), bf16[16,192,256]{2,1,0:T(8,128)(2,1)S(1)}, u32[]{:S(2)}, u32[]{:S(2)}) async-start(bf16[16,192,256]{2,1,0:T(8,128)(2,1)} %bitcast.84), calls=%async_computation.10 | async-start | bytes 3145728 | tf_op jit(solution)/shard_map/all_to_all | solution.py:14
  308.6 57.3 %copy-start.1 = (bf16[1536,256]{1,0:T(8,128)(2,1)S(1)}, bf16[1536,256]{1,0:T(8,128)(2,1)}, u32[]{:S(2)}) copy-start(bf16[1536,256]{1,0:T(8,128)(2,1)} %param.6) | copy-start | bytes 2359300
  353.0 11.7 %collective-permute-start.2 = (bf16[768,256]{1,0:T(8,128)(2,1)S(1)}, bf16[768,256]{1,0:T(8,128)(2,1)S(1)}, u32[]{:S(2)}, u32[]{:S(2)}) collective-permute-start(bf16[768,256]{1,0:T(8,128)(2,1)S(1)} %bitcast.97), channel_id=1, source_target_pairs={{0,1},{1,0},{2,3},{3,2},{4,5},{5,4},{6,7},{7,6},{8,9},{9,8},{10,11... | collective-permute-start | bytes 1179656 | tf_op jit(solution)/shard_map/ppermute | solution.py:22
where the time goes:
time: 367 us; the launch traced here: 366 us
  blocking collectives  177 us (48%)
  waiting for transfers between devices  76.9 us (21%)
  starting transfers between devices  52.9 us (14%)
  local copies, waits for them, and re-layouts  31.9 us (9%)
  matrix products  18.1 us (5%)
  other arithmetic  8.87 us (2%)
    all_to_all x6, blocking collectives, exchange(): return lax.all_to_all(parts, axes, 0, 0, tiled=True)  119 us
    all_to_all x6, waiting for transfers between devices, exchange(): return lax.all_to_all(parts, axes, 0, 0, tiled=True)  75.6 us
    all_to_all x6, starting transfers between devices, exchange(): return lax.all_to_all(parts, axes, 0, 0, tiled=True)  32.1 us
    psum x1, blocking collectives, per_device(): lax.psum(jnp.stack((mixed.sum(axis=1), (mixed * mixed).sum(axis=1))), ('z...  31.9 us
    ppermute x3, starting transfers between devices, swap_core(): return lax.ppermute(block, 'c', [(0, 1), (1, 0)])  20.8 us
    all_gather x1, blocking collectives, per_device(): affine = lax.all_gather(affine, 'x', axis=1, tiled=True)  18.8 us
    dot_general x2, matrix products, dot_nt(): lax.dot_general(a, b, (((1,), (1,)), ((), ())), preferred_element_type=F32)  9.85 us
  transfers between devices with their start and end apart: 9, of which 6 were waited for; matrix products, arithmetic and copies ran while one was open for 6% of the time, Pallas kernels for 0%

commit v1 on v0

--- a/solution.py
+++ b/solution.py
@@ -80,7 +80,9 @@
     branch = exchange(parts, ("x", "y")).astype(F32).sum(axis=0)
     own = lax.dynamic_slice(stream, (y * quarter, x * 256), (quarter, 256))
     mixed = RESIDUAL * own.astype(F32) + branch
-    stats = lax.psum(jnp.stack((mixed.sum(axis=1), (mixed * mixed).sum(axis=1))), ("z", "x"))
+    stats = lax.psum(
+        lax.psum(jnp.stack((mixed.sum(axis=1), (mixed * mixed).sum(axis=1))), "z"), "x"
+    )
     out = normed(mixed, stats[0], stats[1], norm_gain[1], norm_shift[1])
     ours = share(out, "y", 4).reshape(half, 256)
     theirs = swap_core(ours)

time: 367 us -> 348 us (0.948)
  blocking collectives: 177 us -> 160 us
    psum x1, blocking collectives: 31.9 us -> 8.82 us  [per_device(): lax.psum(lax.psum(jnp.stack((mixed.sum(axis=1), (mixed * mixed).sum(axis=...]
    psum x1 -> x2, blocking collectives: 6.89 us -> 13.8 us  [per_device(): lax.psum(jnp.stack((mixed.sum(axis=1), (mixed * mixed).sum(axis=1))), 'z')]
  transfers between devices with their start and end apart: 9 -> 9, of which waited for: 6 -> 6; matrix products, arithmetic and copies ran while one was open for 6% -> 7% of each run, Pallas kernels for 0% -> 0%
where the time goes in v1:
time: 348 us; the launch traced here: 346 us
  blocking collectives  160 us (46%)
  waiting for transfers between devices  76.8 us (22%)
  starting transfers between devices  49.9 us (14%)
  local copies, waits for them, and re-layouts  31.9 us (9%)
  matrix products  18.1 us (5%)
  other arithmetic  8.87 us (3%)
    all_to_all x6, blocking collectives, exchange(): return lax.all_to_all(parts, axes, 0, 0, tiled=True)  119 us
    all_to_all x6, waiting for transfers between devices, exchange(): return lax.all_to_all(parts, axes, 0, 0, tiled=True)  75.4 us
    all_to_all x6, starting transfers between devices, exchange(): return lax.all_to_all(parts, axes, 0, 0, tiled=True)  32 us
    all_gather x1, blocking collectives, per_device(): affine = lax.all_gather(affine, 'x', axis=1, tiled=True)  18.8 us
    ppermute x3, starting transfers between devices, swap_core(): return lax.ppermute(block, 'c', [(0, 1), (1, 0)])  17.9 us
    psum x2, blocking collectives, per_device(): lax.psum(jnp.stack((mixed.sum(axis=1), (mixed * mixed).sum(axis=1))), 'z')  13.8 us
    dot_general x2, matrix products, dot_nt(): lax.dot_general(a, b, (((1,), (1,)), ((), ())), preferred_element_type=F32)  9.85 us
    psum x1, blocking collectives, per_device(): lax.psum(lax.psum(jnp.stack((mixed.sum(axis=1), (mixed * mixed).sum(axis=...  8.82 us
  transfers between devices with their start and end apart: 9, of which 6 were waited for; matrix products, arithmetic and copies ran while one was open for 7% of the time, Pallas kernels for 0%

profile of v1, /device:TPU:1, one launch (start us, length us, event | category | flops | bytes accessed | tf_op | source)
XLA Modules:
  0.0 346.3 jit_solution(12665493751490253051)
XLA Ops:
  0.0 2.4 fusion.6
  2.4 0.3 copy.37
  2.6 2.3 fusion.7
  4.9 0.3 copy.38
  5.2 2.3 fusion.8
  7.5 0.2 maximum_bitcast_fusion
  7.9 30.5 %all_to_all.60 = bf16[4,3,352,256]{3,2,1,0:T(8,128)(2,1)S(1)} all-to-all(bf16[4,3,352,256]{3,2,1,0:T(8,128)(2,1)S(1)} %copy.30), channel_id=1, replica_groups=mesh['z'=4,'x'=4,'y'=4,'c'=2] {'x'}, dimensions={0} | all-to-all | bytes 4325376 | tf_op jit(solution)/shard_map/all_to_all | solution.py:14
  38.4 0.3 copy.42
  38.7 2.2 collective-permute-start
  40.9 10.2 %all_to_all.61 = bf16[4,192,256]{2,1,0:T(8,128)(2,1)S(1)} all-to-all(bf16[4,192,256]{2,1,0:T(8,128)(2,1)S(1)} %broadcast_in_dim.14), channel_id=1, replica_groups=mesh['z'=4,'x'=4,'y'=4,'c'=2] {'x'}, dimensions={0} | all-to-all | bytes 786432 | tf_op jit(solution)/shard_map/all_to_all | solution.py:14
  51.2 1.4 broadcast_in_dim.16
  52.6 4.3 %all-to-all-start.1 = ((bf16[4,192,1024]{2,1,0:T(8,128)(2,1)}), bf16[4,192,1024]{2,1,0:T(8,128)(2,1)}, u32[]{:S(2)}, u32[]{:S(2)}) async-start(bf16[4,192,1024]{2,1,0:T(8,128)(2,1)} %broadcast_in_dim.16), calls=%async_computation.1 | async-start | bytes 3145728 | tf_op jit(solution)/shard_map/all_to_all | solution.py:14
  57.2 1.8 constant_dynamic-update-slice_fusion
  59.0 2.1 copy-done.2
  61.0 1.9 slice.96
  62.9 13.6 %all-to-all-done.1 = bf16[4,192,1024]{2,1,0:T(8,128)(2,1)} async-done(((bf16[4,192,1024]{2,1,0:T(8,128)(2,1)}), bf16[4,192,1024]{2,1,0:T(8,128)(2,1)}, u32[]{:S(2)}, u32[]{:S(2)}) %all-to-all-start.1) | async-done | bytes 1572896 | tf_op jit(solution)/shard_map/all_to_all | solution.py:14
  76.5 4.9 %convolution_convert_fusion.1 = bf16[768,1408]{1,0:T(8,128)(2,1)S(1)} fusion(bf16[768,1024]{1,0:T(8,128)(2,1)} %bitcast.1, bf16[1408,1024]{1,0:T(8,128)(2,1)} %bitcast.85), kind=kOutput, calls=%fused_computation.3 | convolution fusion | flops 2215673856 | bytes 6619136 | tf_op jit(solution)/shard_map/dot_general | solution.py:26
  81.4 29.2 %all_to_all.62 = bf16[4,192,1408]{2,1,0:T(8,128)(2,1)S(1)} all-to-all(bf16[4,192,1408]{2,1,0:T(8,128)(2,1)S(1)} %bitcast.93), channel_id=1, replica_groups=mesh['z'=4,'x'=4,'y'=4,'c'=2] {'z'}, dimensions={0} | all-to-all | bytes 4325376 | tf_op jit(solution)/shard_map/all_to_all | solution.py:14
  110.6 0.3 convert_reduce_fusion.1
  110.9 0.2 fusion.1
  111.1 1.2 broadcast_in_dim.17
  112.3 4.4 %all-to-all-start.4 = ((bf16[4,192,704]{2,1,0:T(8,128)(2,1)}), bf16[4,192,704]{2,1,0:T(8,128)(2,1)}, u32[]{:S(2)}, u32[]{:S(2)}) async-start(bf16[4,192,704]{2,1,0:T(8,128)(2,1)} %broadcast_in_dim.17), calls=%async_computation.4 | async-start | bytes 2359296 | tf_op jit(solution)/shard_map/all_to_all | solution.py:14
  116.7 0.3 copy.39
  117.0 0.3 copy.40
  117.3 0.2 maximum_bitcast_fusion.1
  117.6 1.5 copy.34
  119.1 10.4 %all-to-all-done.4 = bf16[4,192,704]{2,1,0:T(8,128)(2,1)} async-done(((bf16[4,192,704]{2,1,0:T(8,128)(2,1)}), bf16[4,192,704]{2,1,0:T(8,128)(2,1)}, u32[]{:S(2)}, u32[]{:S(2)}) %all-to-all-start.4) | async-done | bytes 1081376 | tf_op jit(solution)/shard_map/all_to_all | solution.py:14
  129.4 3.6 %all-to-all-start.7 = ((bf16[4,3,352,256]{3,2,1,0:T(8,128)(2,1)}), bf16[4,3,352,256]{3,2,1,0:T(8,128)(2,1)S(1)}, u32[]{:S(2)}, u32[]{:S(2)}) async-start(bf16[4,3,352,256]{3,2,1,0:T(8,128)(2,1)} %copy.34), calls=%async_computation.7 | async-start | bytes 4325376 | tf_op jit(solution)/shard_map/all_to_all | solution.py:14
  133.1 4.3 %convolution_convert_fusion.3 = bf16[768,1024]{1,0:T(8,128)(2,1)} fusion(bf16[768,704]{1,0:T(8,128)(2,1)} %bitcast.13, bf16[3,704,1024]{2,1,0:T(8,128)(2,1)} %copy-done.2), kind=kOutput, calls=%fused_computation.9 | convolution fusion | flops 1108082688 | bytes 4194304 | tf_op jit(solution)/shard_map/dot_general | solution.py:69
  137.4 18.0 %all-to-all-done.7 = bf16[4,3,352,256]{3,2,1,0:T(8,128)(2,1)S(1)} async-done(((bf16[4,3,352,256]{3,2,1,0:T(8,128)(2,1)}), bf16[4,3,352,256]{3,2,1,0:T(8,128)(2,1)S(1)}, u32[]{:S(2)}, u32[]{:S(2)}) %all-to-all-start.7) | async-done | bytes 2162720 | tf_op jit(solution)/shard_map/all_to_all | solution.py:14
  155.3 4.4 %all-to-all-start.5 = ((bf16[16,48,1024]{2,1,0:T(8,128)(2,1)}), bf16[16,48,1024]{2,1,0:T(8,128)(2,1)}, u32[]{:S(2)}, u32[]{:S(2)}) async-start(bf16[16,48,1024]{2,1,0:T(8,128)(2,1)} %bitcast.95), calls=%async_computation.5 | async-start | bytes 3145728 | tf_op jit(solution)/shard_map/all_to_all | solution.py:14
  159.8 18.8 %all_gather.3 = f32[2,1024]{1,0:T(2,128)S(1)} all-gather(f32[2,256]{1,0:T(2,128)S(1)} %pad_maximum_fusion), channel_id=1, replica_groups=mesh['z'=4,'x'=4,'y'=4,'c'=2] {'x'}, dimensions={1}, use_global_device_ids=true | all-gather | bytes 10240 | tf_op jit(solution)/shard_map/all_gather | solution.py:65
  178.6 1.6 copy.43
  180.3 8.3 %collective-permute-start.1 = (bf16[3,352,1024]{2,1,0:T(8,128)(2,1)}, bf16[3,352,1024]{2,1,0:T(8,128)(2,1)S(1)}, u32[]{:S(2)}, u32[]{:S(2)}) collective-permute-start(bf16[3,352,1024]{2,1,0:T(8,128)(2,1)} %bitcast.59), channel_id=1, source_target_pairs={{0,1},{1,0},{2,3},{3,2},{4,5},{5,4},{6,7},{7,6},{8,9},{9,8},{10,11... | collective-permute-start | bytes 6488072 | tf_op jit(solution)/shard_map/ppermute | solution.py:22
  188.6 1.7 convert_reduce_fusion.3
  190.3 1.0 fusion.2
  191.4 6.9 %psum.21 = f32[2,48]{1,0:T(2,128)S(1)} all-reduce(f32[2,48]{1,0:T(2,128)S(1)} %pad_maximum_fusion.2), channel_id=1, replica_groups=mesh['z'=4,'x'=4,'y'=4,'c'=2] {'z'}, use_global_device_ids=true, to_apply=%region_4.5 | all-reduce | flops 96 | bytes 768 | tf_op jit(solution)/shard_map/psum | solution.py:74
  198.3 1.0 add_convert_fusion.1
  199.3 1.4 broadcast_in_dim.18
  200.7 5.1 %all-to-all-start.6 = ((bf16[16,48,1024]{2,1,0:T(8,128)(2,1)}), bf16[16,48,1024]{2,1,0:T(8,128)(2,1)}, u32[]{:S(2)}, u32[]{:S(2)}) async-start(bf16[16,48,1024]{2,1,0:T(8,128)(2,1)} %broadcast_in_dim.18), calls=%async_computation.6 | async-start | bytes 3145728 | tf_op jit(solution)/shard_map/all_to_all | solution.py:14
  205.7 1.8 constant_dynamic-update-slice_fusion.3
  207.5 0.2 constant_dynamic-update-slice_fusion.2
  207.7 2.0 copy-done.3
  209.8 1.9 slice.102
  211.7 14.5 %all-to-all-done.6 = bf16[16,48,1024]{2,1,0:T(8,128)(2,1)} async-done(((bf16[16,48,1024]{2,1,0:T(8,128)(2,1)}), bf16[16,48,1024]{2,1,0:T(8,128)(2,1)}, u32[]{:S(2)}, u32[]{:S(2)}) %all-to-all-start.6) | async-done | bytes 1572896 | tf_op jit(solution)/shard_map/all_to_all | solution.py:14
  226.2 4.9 %convolution_convert_fusion = bf16[768,1408]{1,0:T(8,128)(2,1)S(1)} fusion(bf16[768,1024]{1,0:T(8,128)(2,1)} %bitcast.22, bf16[1408,1024]{1,0:T(8,128)(2,1)} %bitcast.86), kind=kOutput, calls=%fused_computation.2 | convolution fusion | flops 2215673856 | bytes 6619136 | tf_op jit(solution)/shard_map/dot_general | solution.py:26
  231.1 25.4 %all_to_all.63 = bf16[4,192,1408]{2,1,0:T(8,128)(2,1)S(1)} all-to-all(bf16[4,192,1408]{2,1,0:T(8,128)(2,1)S(1)} %bitcast.94), channel_id=1, replica_groups=mesh['z'=4,'x'=4,'y'=4,'c'=2] {'z'}, dimensions={0} | all-to-all | bytes 4325376 | tf_op jit(solution)/shard_map/all_to_all | solution.py:14
  256.6 0.3 convert_reduce_fusion
  256.9 0.2 fusion
  257.2 13.7 %all_to_all.64 = bf16[4,192,704]{2,1,0:T(8,128)(2,1)S(1)} all-to-all(bf16[4,192,704]{2,1,0:T(8,128)(2,1)S(1)} %broadcast_in_dim.19), channel_id=1, replica_groups=mesh['z'=4,'x'=4,'y'=4,'c'=2] {'z'}, dimensions={0} | all-to-all | bytes 2162688 | tf_op jit(solution)/shard_map/all_to_all | solution.py:14
  271.0 3.9 %convolution_convert_fusion.2 = bf16[768,1024]{1,0:T(8,128)(2,1)} fusion(bf16[768,704]{1,0:T(8,128)(2,1)S(1)} %bitcast.100, bf16[3,704,1024]{2,1,0:T(8,128)(2,1)} %copy-done.3), kind=kOutput, calls=%fused_computation.8 | convolution fusion | flops 1108082688 | bytes 4096000 | tf_op jit(solution)/shard_map/dot_general | solution.py:78
  274.9 2.9 reshape.113
  277.8 1.4 copy.36
  279.2 10.2 %all-to-all-start.10 = ((bf16[16,192,256]{2,1,0:T(8,128)(2,1)}), bf16[16,192,256]{2,1,0:T(8,128)(2,1)S(1)}, u32[]{:S(2)}, u32[]{:S(2)}) async-start(bf16[16,192,256]{2,1,0:T(8,128)(2,1)} %bitcast.84), calls=%async_computation.10 | async-start | bytes 3145728 | tf_op jit(solution)/shard_map/all_to_all | solution.py:14
  289.4 19.0 %all-to-all-done.10 = bf16[16,192,256]{2,1,0:T(8,128)(2,1)S(1)} async-done(((bf16[16,192,256]{2,1,0:T(8,128)(2,1)}), bf16[16,192,256]{2,1,0:T(8,128)(2,1)S(1)}, u32[]{:S(2)}, u32[]{:S(2)}) %all-to-all-start.10) | async-done | bytes 1572896 | tf_op jit(solution)/shard_map/all_to_all | solution.py:14
  308.4 0.2 convert_reduce_fusion.2
  308.7 1.1 fusion.3
  309.8 6.9 %psum.22 = f32[2,192]{1,0:T(2,128)S(1)} all-reduce(f32[2,192]{1,0:T(2,128)S(1)} %pad_maximum_fusion.1), channel_id=1, replica_groups=mesh['z'=4,'x'=4,'y'=4,'c'=2] {'z'}, use_global_device_ids=true, to_apply=%region_9.10 | all-reduce | flops 384 | bytes 3072 | tf_op jit(solution)/shard_map/psum | solution.py:84
  316.6 8.8 %psum.23 = f32[2,192]{1,0:T(2,128)S(1)} all-reduce(f32[2,192]{1,0:T(2,128)S(1)} %psum.22), channel_id=1, replica_groups=mesh['z'=4,'x'=4,'y'=4,'c'=2] {'x'}, use_global_device_ids=true, to_apply=%region_10.11 | all-reduce | flops 384 | bytes 3072 | tf_op jit(solution)/shard_map/psum | solution.py:83
  325.5 1.0 add_convert_fusion
  326.5 9.8 %all_to_all.65 = bf16[4,192,256]{2,1,0:T(8,128)(2,1)S(1)} all-to-all(bf16[4,192,256]{2,1,0:T(8,128)(2,1)S(1)} %broadcast_in_dim.20), channel_id=1, replica_groups=mesh['z'=4,'x'=4,'y'=4,'c'=2] {'y'}, dimensions={0} | all-to-all | bytes 786432 | tf_op jit(solution)/shard_map/all_to_all | solution.py:14
  336.4 7.4 %collective-permute-start.2 = (bf16[768,256]{1,0:T(8,128)(2,1)S(1)}, bf16[768,256]{1,0:T(8,128)(2,1)S(1)}, u32[]{:S(2)}, u32[]{:S(2)}) collective-permute-start(bf16[768,256]{1,0:T(8,128)(2,1)S(1)} %bitcast.97), channel_id=1, source_target_pairs={{0,1},{1,0},{2,3},{3,2},{4,5},{5,4},{6,7},{7,6},{8,9},{9,8},{10,11... | collective-permute-start | bytes 1179656 | tf_op jit(solution)/shard_map/ppermute | solution.py:22
  343.8 1.3 collective-permute-done.2
  345.1 1.2 maximum_select_fusion
  (35 shorter events, 0.6 us)
Async XLA Ops:
  0.0 40.9 %copy-start = (bf16[1536,256]{1,0:T(8,128)(2,1)S(1)}, bf16[1536,256]{1,0:T(8,128)(2,1)}, u32[]{:S(2)}) copy-start(bf16[1536,256]{1,0:T(8,128)(2,1)} %param.6) | copy-start | bytes 2359300
  38.7 18.5 %collective-permute-start = (bf16[3,352,1024]{2,1,0:T(8,128)(2,1)S(1)}, bf16[3,352,1024]{2,1,0:T(8,128)(2,1)}, u32[]{:S(2)}, u32[]{:S(2)}) collective-permute-start(bf16[3,352,1024]{2,1,0:T(8,128)(2,1)S(1)} %bitcast.81), channel_id=1, source_target_pairs={{0,1},{1,0},{2,3},{3,2},{4,5},{5,4},{6,7},{7,6},{8,9},{9,8},{10,11... | collective-permute-start | bytes 6488072 | tf_op jit(solution)/shard_map/ppermute | solution.py:22
  52.6 23.8 %all-to-all-start.1 = ((bf16[4,192,1024]{2,1,0:T(8,128)(2,1)}), bf16[4,192,1024]{2,1,0:T(8,128)(2,1)}, u32[]{:S(2)}, u32[]{:S(2)}) async-start(bf16[4,192,1024]{2,1,0:T(8,128)(2,1)} %broadcast_in_dim.16), calls=%async_computation.1 | async-start | bytes 3145728 | tf_op jit(solution)/shard_map/all_to_all | solution.py:14
  59.0 2.1 copy-start.2
  111.1 5.6 %copy-start.4 = (bf16[1,256,1408]{2,1,0:T(8,128)(2,1)S(1)}, bf16[1,256,1408]{2,1,0:T(8,128)(2,1)}, u32[]{:S(2)}) copy-start(bf16[1,256,1408]{2,1,0:T(8,128)(2,1)} %get-tuple-element.9) | copy-start | bytes 2162692
  112.3 4.7 %copy-start.5 = (bf16[1,256,1408]{2,1,0:T(8,128)(2,1)S(1)}, bf16[1,256,1408]{2,1,0:T(8,128)(2,1)}, u32[]{:S(2)}) copy-start(bf16[1,256,1408]{2,1,0:T(8,128)(2,1)} %get-tuple-element.11) | copy-start | bytes 2162692
  112.3 5.0 %copy-start.6 = (bf16[1,1408,256]{2,1,0:T(8,128)(2,1)S(1)}, bf16[1,1408,256]{2,1,0:T(8,128)(2,1)}, u32[]{:S(2)}) copy-start(bf16[1,1408,256]{2,1,0:T(8,128)(2,1)} %get-tuple-element.13) | copy-start | bytes 2162692
  112.3 17.1 %all-to-all-start.4 = ((bf16[4,192,704]{2,1,0:T(8,128)(2,1)}), bf16[4,192,704]{2,1,0:T(8,128)(2,1)}, u32[]{:S(2)}, u32[]{:S(2)}) async-start(bf16[4,192,704]{2,1,0:T(8,128)(2,1)} %broadcast_in_dim.17), calls=%async_computation.4 | async-start | bytes 2359296 | tf_op jit(solution)/shard_map/all_to_all | solution.py:14
  129.4 25.9 %all-to-all-start.7 = ((bf16[4,3,352,256]{3,2,1,0:T(8,128)(2,1)}), bf16[4,3,352,256]{3,2,1,0:T(8,128)(2,1)S(1)}, u32[]{:S(2)}, u32[]{:S(2)}) async-start(bf16[4,3,352,256]{3,2,1,0:T(8,128)(2,1)} %copy.34), calls=%async_computation.7 | async-start | bytes 4325376 | tf_op jit(solution)/shard_map/all_to_all | solution.py:14
  137.4 22.4 %copy-start.7 = (f32[2,256]{1,0:T(2,128)S(1)}, f32[2,256]{1,0:T(2,128)}, u32[]{:S(2)}) copy-start(f32[2,256]{1,0:T(2,128)} %param.10) | copy-start | bytes 6148
  137.4 22.4 %copy-start.8 = (f32[2,256]{1,0:T(2,128)S(1)}, f32[2,256]{1,0:T(2,128)}, u32[]{:S(2)}) copy-start(f32[2,256]{1,0:T(2,128)} %param.11) | copy-start | bytes 6148
  155.3 33.2 %all-to-all-start.5 = ((bf16[16,48,1024]{2,1,0:T(8,128)(2,1)}), bf16[16,48,1024]{2,1,0:T(8,128)(2,1)}, u32[]{:S(2)}, u32[]{:S(2)}) async-start(bf16[16,48,1024]{2,1,0:T(8,128)(2,1)} %bitcast.95), calls=%async_computation.5 | async-start | bytes 3145728 | tf_op jit(solution)/shard_map/all_to_all | solution.py:14
  180.3 27.3 %collective-permute-start.1 = (bf16[3,352,1024]{2,1,0:T(8,128)(2,1)}, bf16[3,352,1024]{2,1,0:T(8,128)(2,1)S(1)}, u32[]{:S(2)}, u32[]{:S(2)}) collective-permute-start(bf16[3,352,1024]{2,1,0:T(8,128)(2,1)} %bitcast.59), channel_id=1, source_target_pairs={{0,1},{1,0},{2,3},{3,2},{4,5},{5,4},{6,7},{7,6},{8,9},{9,8},{10,11... | collective-permute-start | bytes 6488072 | tf_op jit(solution)/shard_map/ppermute | solution.py:22
  200.7 25.6 %all-to-all-start.6 = ((bf16[16,48,1024]{2,1,0:T(8,128)(2,1)}), bf16[16,48,1024]{2,1,0:T(8,128)(2,1)}, u32[]{:S(2)}, u32[]{:S(2)}) async-start(bf16[16,48,1024]{2,1,0:T(8,128)(2,1)} %broadcast_in_dim.18), calls=%async_computation.6 | async-start | bytes 3145728 | tf_op jit(solution)/shard_map/all_to_all | solution.py:14
  207.7 2.0 copy-start.3
  279.2 29.2 %all-to-all-start.10 = ((bf16[16,192,256]{2,1,0:T(8,128)(2,1)}), bf16[16,192,256]{2,1,0:T(8,128)(2,1)S(1)}, u32[]{:S(2)}, u32[]{:S(2)}) async-start(bf16[16,192,256]{2,1,0:T(8,128)(2,1)} %bitcast.84), calls=%async_computation.10 | async-start | bytes 3145728 | tf_op jit(solution)/shard_map/all_to_all | solution.py:14
  308.4 37.8 %copy-start.1 = (bf16[1536,256]{1,0:T(8,128)(2,1)S(1)}, bf16[1536,256]{1,0:T(8,128)(2,1)}, u32[]{:S(2)}) copy-start(bf16[1536,256]{1,0:T(8,128)(2,1)} %param.6) | copy-start | bytes 2359300
  336.4 8.7 %collective-permute-start.2 = (bf16[768,256]{1,0:T(8,128)(2,1)S(1)}, bf16[768,256]{1,0:T(8,128)(2,1)S(1)}, u32[]{:S(2)}, u32[]{:S(2)}) collective-permute-start(bf16[768,256]{1,0:T(8,128)(2,1)S(1)} %bitcast.97), channel_id=1, source_target_pairs={{0,1},{1,0},{2,3},{3,2},{4,5},{5,4},{6,7},{7,6},{8,9},{9,8},{10,11... | collective-permute-start | bytes 1179656 | tf_op jit(solution)/shard_map/ppermute | solution.py:22
